TPU v7x, 32 devices: a whole 2x2x4 slice. The times are simulated.
32 devices in a mesh: ep: 8 (over z, x), tp: 4 (over y, core).
Axes of the slice: x: 2, y: 2, z: 4, core: 2. Of those that a mesh axis runs over, the one named last changes fastest.
Arguments:
- hidden_in: bfloat16 [128, 2048], P(None, 'ep'), may hold values from -24 to 24
- attn_gain: float32 [2048], replicated, may hold values from 0.1 to 1.9
- forget_weight: bfloat16 [2048, 16], replicated, may hold values from -0.125 to 0.125
- forget_bias: float32 [16], replicated, may hold values from -1 to 2
- query_weight: bfloat16 [2048, 2048], P('ep', 'tp'), may hold values from -0.125 to 0.125
- key_weight: bfloat16 [2048, 1024], P('ep', 'tp'), may hold values from -0.125 to 0.125
- value_weight: bfloat16 [2048, 1024], P('ep', 'tp'), may hold values from -0.125 to 0.125
- query_gain: float32 [128], replicated, may hold values from 0.1 to 1.9
- key_gain: float32 [128], replicated, may hold values from 0.1 to 1.9
- cache_keys: bfloat16 [128, 8, 1024, 128], P('ep', 'tp'), may hold values from -160 to 160
- cache_values: bfloat16 [128, 8, 1024, 128], P('ep', 'tp'), may hold values from -6 to 6
- cache_gates: float32 [128, 16, 1024], P('ep', 'tp'), may hold values from -256 to 0, as said below
- lengths: int32 [128], P('ep'), may hold values from 128 to 1024, as said below
- output_weight: bfloat16 [2048, 2048], P('tp', 'ep'), may hold values from -0.125 to 0.125
- ffn_gain: float32 [2048], replicated, may hold values from 0.1 to 1.9
- route_group: int32 [128], replicated, may hold values from 0 to 3, as said below
- route_expert: int32 [128, 2], replicated, may hold values from 0 to 3, as said below
- route_weight: float32 [128, 2], replicated, may hold values from 0.1 to 0.6
- expert_gate: bfloat16 [16, 2048, 1024], P('ep', None, 'tp'), may hold values from -0.125 to 0.125
- expert_up: bfloat16 [16, 2048, 1024], P('ep', None, 'tp'), may hold values from -0.125 to 0.125
- expert_down: bfloat16 [16, 1024, 2048], P('ep', 'tp'), may hold values from -0.1875 to 0.1875
- mix_vector: bfloat16 [2048], replicated, may hold values from -0.125 to 0.125
- dense_gate: bfloat16 [2048, 4096], P('ep', 'tp'), may hold values from -0.125 to 0.125
- dense_up: bfloat16 [2048, 4096], P('ep', 'tp'), may hold values from -0.125 to 0.125
- dense_down: bfloat16 [4096, 2048], P('tp', 'ep'), may hold values from -0.09375 to 0.09375
Outputs:
- mixed: bfloat16 [128, 2048], P(None, 'ep')
- fresh_keys: bfloat16 [128, 1024], P('ep', 'tp')
- fresh_values: bfloat16 [128, 1024], P('ep', 'tp')
Inputs may be any that keep to these rules, and one draw needn't show every extreme that they name: `cache_gates`: never rising along positions. `lengths`: some device holds a sequence of length 1024 in every draw. `route_group`: no expert is chosen by more than 24 tokens of the batch, and some expert by exactly 24. `route_expert`: a token's 2 experts differ; the loads of the experts of one group differ by at most two.
All inputs are finite; a program needn't handle non-finite values.
Results may differ from a plain program's by a relative error of at most 0.008.
Values may be sent and summed in bfloat16 or wider, within the bound.
A program may use at most 64 MiB of HBM per device.

v0:
```python
import jax
import jax.numpy as jnp
from jax import lax
from jax.sharding import PartitionSpec as P

D = 2048
HEAD_DIM = 128
GROUP_EXPERTS = 4
TOPK = 2
CAPACITY = 24
EPS = 1e-06


def head_norm(projected, gain_vec):
    return (
        projected
        * lax.rsqrt(jnp.mean(projected * projected, axis=-1, keepdims=True) + EPS)
        * gain_vec
    )


def slot_targets(route_group, route_expert, expert_count):
    chosen = (route_group[:, None] * GROUP_EXPERTS + route_expert).reshape(-1)
    onehot = (chosen[:, None] == jnp.arange(expert_count, dtype=jnp.int32)[None, :]).astype(
        jnp.int32
    )
    before = jnp.cumsum(onehot, axis=0) - onehot
    return chosen * CAPACITY + jnp.sum(before * onehot, axis=1)


def on_device(
    hidden_in,
    attn_gain,
    forget_weight,
    forget_bias,
    query_weight,
    key_weight,
    value_weight,
    query_gain,
    key_gain,
    cache_keys,
    cache_values,
    cache_gates,
    lengths,
    output_weight,
    ffn_gain,
    route_group,
    route_expert,
    route_weight,
    expert_gate,
    expert_up,
    expert_down,
    mix_vector,
    dense_gate,
    dense_up,
    dense_down,
):
    seq_count, width_block = hidden_in.shape
    own_count = cache_keys.shape[0]
    ep_index = lax.axis_index("ep")
    tp_index = lax.axis_index("tp")
    ep_count = lax.axis_size("ep")
    col_start = ep_index * width_block
    row_start = ep_index * own_count
    stream = hidden_in.astype(jnp.float32)
    normed_in = (stream * lax.dynamic_slice_in_dim(attn_gain, col_start, width_block)).astype(
        jnp.bfloat16
    )
    forget_rows = lax.dynamic_slice_in_dim(forget_weight, col_start, width_block, 0)
    squares, forget_dot = lax.psum(
        (
            jnp.sum(stream * stream, axis=1),
            jnp.dot(normed_in, forget_rows, preferred_element_type=jnp.float32),
        ),
        "ep",
    )
    inv_rms = lax.rsqrt(squares / D + EPS)
    query_cols = query_weight.shape[1]
    key_cols = key_weight.shape[1]
    selected = normed_in
    head_sums = lax.psum_scatter(
        jnp.concatenate(
            [
                jnp.dot(selected, query_weight, preferred_element_type=jnp.float32),
                jnp.dot(selected, key_weight, preferred_element_type=jnp.float32),
                jnp.dot(selected, value_weight, preferred_element_type=jnp.float32),
            ],
            axis=1,
        ),
        "ep",
        scatter_dimension=0,
        tiled=True,
    )
    heads_here = query_cols // HEAD_DIM
    kv_here = key_cols // HEAD_DIM
    group_size = heads_here // kv_here
    own_scale = lax.dynamic_slice_in_dim(inv_rms, row_start, own_count)
    query_rows = head_norm(
        head_sums[:, :query_cols].reshape(own_count, heads_here, HEAD_DIM), query_gain
    ).astype(jnp.bfloat16)
    fresh_key = head_norm(
        head_sums[:, query_cols : query_cols + key_cols].reshape(own_count, kv_here, HEAD_DIM),
        key_gain,
    ).astype(jnp.bfloat16)
    fresh_value = (head_sums[:, query_cols + key_cols :] * own_scale[:, None]).astype(jnp.bfloat16)
    gate_logit = lax.dynamic_slice(
        forget_dot, (row_start, tp_index * heads_here), (own_count, heads_here)
    )
    bias_here = lax.dynamic_slice_in_dim(forget_bias, tp_index * heads_here, heads_here)
    log_forget = jax.nn.log_sigmoid(gate_logit * own_scale[:, None] + bias_here)
    latest = jnp.take_along_axis(cache_gates, (lengths - 1)[:, None, None], axis=2)[:, :, 0]
    now_gate = (latest + log_forget).reshape(own_count, kv_here, group_size)
    grouped = query_rows.reshape(own_count, kv_here, group_size, HEAD_DIM)
    factor = HEAD_DIM ** (-0.5)
    scores = (
        jnp.einsum("skgd,skcd->skgc", grouped, cache_keys, preferred_element_type=jnp.float32)
        * factor
    )
    scores = scores + now_gate[..., None] - cache_gates.reshape(own_count, kv_here, group_size, -1)
    in_cache = (
        jnp.arange(cache_keys.shape[2], dtype=jnp.int32)[None, None, None, :]
        < lengths[:, None, None, None]
    )
    scores = jnp.where(in_cache, scores, -jnp.inf)
    self_score = (
        jnp.einsum("skgd,skd->skg", grouped, fresh_key, preferred_element_type=jnp.float32) * factor
    )
    ceiling = jnp.maximum(jnp.max(scores, axis=-1), self_score)
    weights = jnp.exp(scores - ceiling[..., None])
    self_weight = jnp.exp(self_score - ceiling)
    denominator = jnp.sum(weights, axis=-1) + self_weight
    mixed_heads = jnp.einsum(
        "skgc,skcd->skgd",
        weights.astype(jnp.bfloat16),
        cache_values,
        preferred_element_type=jnp.float32,
    )
    mixed_heads = mixed_heads + self_weight[..., None] * fresh_value.reshape(
        own_count, kv_here, 1, HEAD_DIM
    ).astype(jnp.float32)
    heads_out = (
        (mixed_heads / denominator[..., None]).reshape(own_count, query_cols).astype(jnp.bfloat16)
    )
    attn_part = jnp.dot(
        lax.all_gather(heads_out, "ep", axis=0, tiled=True),
        output_weight,
        preferred_element_type=jnp.float32,
    )
    attn_out = lax.psum(attn_part, "tp")
    middle = (stream + attn_out).astype(jnp.bfloat16).astype(jnp.float32)
    normed_mid = (middle * lax.dynamic_slice_in_dim(ffn_gain, col_start, width_block)).astype(
        jnp.bfloat16
    )
    mix_part = jnp.dot(
        normed_mid,
        lax.dynamic_slice_in_dim(mix_vector, col_start, width_block),
        preferred_element_type=jnp.float32,
    )
    squares_mid, mix_dot = lax.psum((jnp.sum(middle * middle, axis=1), mix_part), "ep")
    mid_scale = lax.rsqrt(squares_mid / D + EPS)
    mix_share = jax.nn.sigmoid(mid_scale * mix_dot)
    local_experts = expert_gate.shape[0]
    expert_count = local_experts * ep_count
    targets = slot_targets(route_group, route_expert, expert_count)
    slot_total = expert_count * CAPACITY
    slot_ids = jnp.arange(slot_total, dtype=jnp.int32)
    placed = jnp.any(
        targets.reshape(seq_count, TOPK)[None, :, :] == slot_ids[:, None, None], axis=2
    )
    outgoing = jnp.dot(placed.astype(jnp.bfloat16), normed_mid, preferred_element_type=jnp.float32)
    outgoing = outgoing.astype(jnp.bfloat16).reshape(ep_count, local_experts, CAPACITY, width_block)
    arrived = lax.all_to_all(outgoing, "ep", split_axis=0, concat_axis=3, tiled=True).reshape(
        local_experts, CAPACITY, -1
    )
    my_slots = lax.dynamic_slice_in_dim(
        placed, ep_index * local_experts * CAPACITY, local_experts * CAPACITY, 0
    )
    slot_scale = jnp.sum(jnp.where(my_slots, mid_scale[None, :], 0.0), axis=1).reshape(
        local_experts, CAPACITY, 1
    )
    gate_pre = (
        jnp.einsum("ecd,edf->ecf", arrived, expert_gate, preferred_element_type=jnp.float32)
        * slot_scale
    )
    up_pre = (
        jnp.einsum("ecd,edf->ecf", arrived, expert_up, preferred_element_type=jnp.float32)
        * slot_scale
    )
    expert_hidden = (jax.nn.silu(gate_pre) * up_pre).astype(jnp.bfloat16)
    expert_part = jnp.einsum(
        "ecf,efd->ecd", expert_hidden, expert_down, preferred_element_type=jnp.float32
    )
    returned = (
        lax.all_to_all(
            expert_part[None].astype(jnp.bfloat16), "ep", split_axis=3, concat_axis=0, tiled=True
        )
        .astype(jnp.float32)
        .reshape(slot_total, width_block)
    )
    picked = jnp.take(returned, targets, axis=0).reshape(seq_count, TOPK, width_block)
    routed = jnp.sum(picked * route_weight[:, :, None], axis=1)
    hidden_width = dense_gate.shape[1]
    selected = normed_mid
    both_sums = lax.psum_scatter(
        jnp.concatenate(
            [
                jnp.dot(selected, dense_gate, preferred_element_type=jnp.float32),
                jnp.dot(selected, dense_up, preferred_element_type=jnp.float32),
            ],
            axis=1,
        ),
        "ep",
        scatter_dimension=0,
        tiled=True,
    )
    gate_sum = both_sums[:, :hidden_width]
    up_sum = both_sums[:, hidden_width:]
    own_mid = lax.dynamic_slice_in_dim(mid_scale, row_start, own_count)
    dense_hidden = (jax.nn.silu(gate_sum * own_mid[:, None]) * (up_sum * own_mid[:, None])).astype(
        jnp.bfloat16
    )
    dense_part = jnp.dot(
        lax.all_gather(dense_hidden, "ep", axis=0, tiled=True),
        dense_down,
        preferred_element_type=jnp.float32,
    )
    ffn_total = lax.psum(
        (routed + mix_share[:, None] * dense_part).astype(jnp.bfloat16), "tp"
    ).astype(jnp.float32)
    mixed = (middle + ffn_total).astype(jnp.bfloat16)
    return (mixed, fresh_key.reshape(own_count, key_cols), fresh_value)


def solution(mesh):
    placed = (
        P(None, "ep"),
        P(),
        P(),
        P(),
        P("ep", "tp"),
        P("ep", "tp"),
        P("ep", "tp"),
        P(),
        P(),
        P("ep", "tp", None, None),
        P("ep", "tp", None, None),
        P("ep", "tp", None),
        P("ep"),
        P("tp", "ep"),
        P(),
        P(),
        P(),
        P(),
        P("ep", None, "tp"),
        P("ep", None, "tp"),
        P("ep", "tp", None),
        P(),
        P("ep", "tp"),
        P("ep", "tp"),
        P("tp", "ep"),
    )
    return jax.shard_map(
        on_device,
        mesh=mesh,
        in_specs=placed,
        out_specs=(P(None, "ep"), P("ep", "tp"), P("ep", "tp")),
        check_vma=False,
    )
```

profile of v0, /device:TPU:0, one launch (start us, length us, event | category | flops | bytes accessed | tf_op | source)
XLA Modules:
  0.0 295.3 jit_solution(9477003200772531910)
XLA Ops:
  8.2 1.2 fusion.40
  9.4 1.1 fusion.36
  10.5 1.1 fusion.38
  13.6 23.6 %all-reduce.1 = (f32[128,16]{0,1:T(8,128)S(1)}, f32[128]{0:T(128)S(1)}) all-reduce(f32[128,16]{0,1:T(8,128)S(1)} %fusion.34, f32[128]{0:T(128)S(1)} %fusion.15), channel_id=1, replica_groups=mesh['ep'=8,'tp'=4] {'ep'}, use_global_device_ids=true, to_apply=%region_2.0 | all-reduce | flops 2176 | bytes 17408 | tf_op jit(solution)/shard_map/psum | solution.py:70
  37.4 4.7 %copy.71 = f32[16,4,1024]{1,2,0:T(8,128)} copy(f32[16,4,1024]{2,1,0:T(4,128)S(1)} %copy-done.4) | data formatting | bytes 524288 | tf_op args[11]
  43.2 1.3 gather_fusion.1
  47.9 30.2 %reduce-scatter.3.cloned.1.call-done = f32[16,1024]{1,0:T(8,128)} async-done(((f32[128,1024]{1,0:T(8,128)}), f32[16,1024]{1,0:T(8,128)}) %reduce-scatter.3.cloned.1.call-update) | async-done | bytes 65552 | tf_op jit(solution)/shard_map/reduce_scatter | solution.py:81
  80.4 5.8 %fusion.64 = (f32[16,2,2]{2,1,0:T(2,128)S(1)}, f32[16,2,2,1024]{3,2,1,0:T(2,128)S(1)}) fusion(f32[16,2,2,1024]{3,2,1,0:T(2,128)S(1)} %reshape.201, f32[16,2,2]{2,1,0:T(2,128)S(1)} %copy.73, bf16[16,2,2,128]{3,2,1,0:T(2,128)(2,1)S(1)} %multiply_convert_fusion, bf16[16,2,1024,128]{3,2,1,0:T(8,128)(2,1)} %param.34, pred[16,1024]{1,0:T(8,128)(4,1)S(1)} %iota_compare_fusion.1), kind=kOutput, calls=%fused_computation.109 | convolution fusion | flops 17104832 | bytes 8946176 | tf_op jit(solution)/shard_map/skgd,skcd->skgc/dot_general | solution.py:116
  87.3 5.4 %fusion.9 = bf16[16,2,2,128]{3,2,1,0:T(2,128)(2,1)} fusion(bf16[16,2,1024,128]{3,2,1,0:T(8,128)(2,1)} %param.35, f32[16,2,2,1024]{3,2,1,0:T(2,128)S(1)} %get-tuple-element.22, f32[16,2,2]{2,1,0:T(2,128)S(1)} %multiply_maximum_fusion, f32[16,2,2]{2,1,0:T(2,128)S(1)} %get-tuple-element.13, f32[16,2,128]{2,1,0:T(2,128)S(1)} %reshape.207, ...), kind=kOutput, calls=%fused_computation.18 | convolution fusion | flops 16941056 | bytes 8684288 | tf_op jit(solution)/shard_map/skgc,skcd->skgd/dot_general | solution.py:132
  93.5 30.5 %all_gather.6 = bf16[128,512]{1,0:T(8,128)(2,1)S(1)} all-gather(bf16[16,512]{1,0:T(8,128)(2,1)S(1)} %convert_element_type.102), channel_id=1, replica_groups=mesh['ep'=8,'tp'=4] {'ep'}, dimensions={0}, use_global_device_ids=true | all-gather | bytes 147456 | tf_op jit(solution)/shard_map/all_gather | solution.py:145
  125.2 30.6 %all-reduce.5.cloned.1.call-done = f32[128,256]{1,0:T(8,128)} async-done(((f32[128,256]{1,0:T(8,128)}), f32[128,256]{1,0:T(8,128)}) %all-reduce.5.cloned.1.call-update) | async-done | bytes 131088 | tf_op jit(solution)/shard_map/psum | solution.py:149
  159.4 5.5 %all-to-all-start = ((bf16[8,2,24,256]{3,2,1,0:T(8,128)(2,1)}), bf16[8,2,24,256]{3,2,1,0:T(8,128)(2,1)S(1)}, u32[]{:S(2)}, u32[]{:S(2)}) async-start(bf16[8,2,24,256]{3,2,1,0:T(8,128)(2,1)} %bitcast.9), calls=%async_computation.1 | async-start | bytes 393216 | tf_op jit(solution)/shard_map/all_to_all | solution.py:172
  165.0 21.9 %all-reduce = (f32[128]{0:T(128)S(1)}, f32[128]{0:T(128)S(1)}) all-reduce(f32[128]{0:T(128)S(1)} %get-tuple-element.11, f32[128]{0:T(128)S(1)} %convolution_bitcast_fusion), channel_id=1, replica_groups=mesh['ep'=8,'tp'=4] {'ep'}, use_global_device_ids=true, to_apply=%region_14.15 | all-reduce | flops 256 | bytes 2048 | tf_op jit(solution)/shard_map/psum | solution.py:159
  187.9 1.9 convolution_multiply_fusion.3
  189.9 2.3 fusion
  193.0 2.0 reshape.232
  195.0 3.4 %all-to-all-start.1 = ((bf16[8,2,6144]{2,1,0:T(2,128)(2,1)}), bf16[8,2,6144]{2,1,0:T(2,128)(2,1)S(1)}, u32[]{:S(2)}, u32[]{:S(2)}) async-start(bf16[8,2,6144]{2,1,0:T(2,128)(2,1)} %reshape.232), calls=%async_computation.2 | async-start | bytes 393216 | tf_op jit(solution)/shard_map/all_to_all | solution.py:194
  201.0 5.2 %all-to-all-done.1 = bf16[8,2,6144]{2,1,0:T(2,128)(2,1)S(1)} async-done(((bf16[8,2,6144]{2,1,0:T(2,128)(2,1)}), bf16[8,2,6144]{2,1,0:T(2,128)(2,1)S(1)}, u32[]{:S(2)}, u32[]{:S(2)}) %all-to-all-start.1) | async-done | bytes 196640 | tf_op jit(solution)/shard_map/all_to_all | solution.py:194
  206.1 1.5 reshape.233
  208.2 1.2 gather_fusion
  210.5 13.5 %reduce-scatter.5.cloned.1.call-done = f32[16,2048]{1,0:T(8,128)} async-done(((f32[128,2048]{1,0:T(8,128)}), f32[16,2048]{1,0:T(8,128)}) %reduce-scatter.5.cloned.1.call-update) | async-done | bytes 131088 | tf_op jit(solution)/shard_map/reduce_scatter | solution.py:204
  225.0 30.9 %all_gather.7 = bf16[128,1024]{1,0:T(8,128)(2,1)S(1)} all-gather(bf16[16,1024]{1,0:T(8,128)(2,1)S(1)} %fusion.22), channel_id=1, replica_groups=mesh['ep'=8,'tp'=4] {'ep'}, dimensions={0}, use_global_device_ids=true | all-gather | bytes 294912 | tf_op jit(solution)/shard_map/all_gather | solution.py:223
  256.7 30.5 %all-reduce.7.cloned.1.call-done = bf16[128,256]{1,0:T(8,128)(2,1)} async-done(((bf16[128,256]{1,0:T(8,128)(2,1)}), bf16[128,256]{1,0:T(8,128)(2,1)}) %all-reduce.7.cloned.1.call-update) | async-done | bytes 65552 | tf_op jit(solution)/shard_map/psum | solution.py:227
  287.3 1.5 fusion.19
  (140 shorter events, 24.2 us)
Async XLA Ops:
  7.2 182.7 %copy-start = (bf16[2,256,2048]{2,1,0:T(8,128)(2,1)S(1)}, bf16[2,256,2048]{2,1,0:T(8,128)(2,1)}, u32[]{:S(2)}) copy-start(bf16[2,256,2048]{2,1,0:T(8,128)(2,1)} %param.45) | copy-start | bytes 6291460
  7.2 30.1 %copy-start.16 = (s32[128,2]{0,1:T(2,128)S(1)}, s32[128,2]{0,1:T(2,128)}, u32[]{:S(2)}) copy-start(s32[128,2]{0,1:T(2,128)} %param.41) | copy-start | bytes 3076
  7.2 30.1 %copy-start.4 = (f32[16,4,1024]{2,1,0:T(4,128)S(1)}, f32[16,4,1024]{2,1,0:T(4,128)}, u32[]{:S(2)}) copy-start(f32[16,4,1024]{2,1,0:T(4,128)} %param.36) | copy-start | bytes 786436
  7.2 70.8 %reduce-scatter.3.cloned.1.call-start = ((), (), s32[]{:S(2)}) async-start(), calls=%async_computation.4 | async-start | bytes 589824 | tf_op jit(solution)/shard_map/reduce_scatter | solution.py:81
  12.5 143.3 %all-reduce.5.cloned.1.call-start = ((), (), s32[]{:S(2)}) async-start(), calls=%async_computation.5 | async-start | bytes 262144 | tf_op jit(solution)/shard_map/psum | solution.py:149
  37.3 7.3 %copy-start.22 = (f32[16]{0:T(128)S(1)}, f32[16]{0:T(128)}, u32[]{:S(2)}) copy-start(f32[16]{0:T(128)} %param.28) | copy-start | bytes 196
  37.3 10.5 %copy-start.17 = (f32[128]{0:T(128)S(1)}, f32[128]{0:T(128)}, u32[]{:S(2)}) copy-start(f32[128]{0:T(128)} %param.33) | copy-start | bytes 1540
  37.4 42.7 %copy-start.18 = (f32[128]{0:T(128)S(1)}, f32[128]{0:T(128)}, u32[]{:S(2)}) copy-start(f32[128]{0:T(128)} %param.32) | copy-start | bytes 1540
  47.8 38.4 %copy-start.12 = (s32[16,3]{0,1:T(4,128)}, s32[16,3]{0,1:T(4,128)S(1)}, u32[]{:S(2)}) copy-start(s32[16,3]{0,1:T(4,128)S(1)} %reduce-window.9) | copy-start | bytes 580
  87.3 36.7 %copy-start.8 = (bf16[512,256]{1,0:T(8,128)(2,1)S(1)}, bf16[512,256]{1,0:T(8,128)(2,1)}, u32[]{:S(2)}) copy-start(bf16[512,256]{1,0:T(8,128)(2,1)} %param.38) | copy-start | bytes 786436
  87.3 37.6 %slice-start = ((s32[16,3]{0,1:T(4,128)}), s32[16,2]{0,1:T(2,128)S(1)}, s32[]{:S(2)}) async-start(s32[16,3]{0,1:T(4,128)} %copy-done.12), calls=%async_computation.8 | async-start | bytes 2048 | tf_op jit(solution)/shard_map/slice.1
  87.3 37.6 %copy-start.13 = (s32[256]{0:T(256)S(1)}, s32[256]{0:T(256)}, u32[]{:S(2)}) copy-start(s32[256]{0:T(256)} %reshape.203) | copy-start | bytes 3076
  87.3 69.5 %copy-start.5 = (bf16[256,1024]{1,0:T(8,128)(2,1)S(1)}, bf16[256,1024]{1,0:T(8,128)(2,1)}, u32[]{:S(2)}) copy-start(bf16[256,1024]{1,0:T(8,128)(2,1)} %param.48) | copy-start | bytes 1572868
  92.7 64.4 %copy-start.6 = (bf16[256,1024]{1,0:T(8,128)(2,1)S(1)}, bf16[256,1024]{1,0:T(8,128)(2,1)}, u32[]{:S(2)}) copy-start(bf16[256,1024]{1,0:T(8,128)(2,1)} %param.47) | copy-start | bytes 1572868
  124.9 99.1 %reduce-scatter.5.cloned.1.call-start = ((), (), s32[]{:S(2)}) async-start(), calls=%async_computation.6 | async-start | bytes 1179648 | tf_op jit(solution)/shard_map/reduce_scatter | solution.py:204
  156.8 8.1 %copy-start.2 = (bf16[128,256]{1,0:T(8,128)(2,1)}, bf16[128,256]{1,0:T(8,128)(2,1)S(1)}, u32[]{:S(2)}) copy-start(bf16[128,256]{1,0:T(8,128)(2,1)S(1)} %get-tuple-element.12) | copy-start | bytes 196612
  157.3 7.6 %copy-start.23 = (bf16[256,1]{0,1:T(2,128)(2,1)S(1)}, bf16[256,1]{0,1:T(2,128)(2,1)}, u32[]{:S(2)}) copy-start(bf16[256,1]{0,1:T(2,128)(2,1)} %reshape.229) | copy-start | bytes 1540
  159.4 28.3 %all-to-all-start = ((bf16[8,2,24,256]{3,2,1,0:T(8,128)(2,1)}), bf16[8,2,24,256]{3,2,1,0:T(8,128)(2,1)S(1)}, u32[]{:S(2)}, u32[]{:S(2)}) async-start(bf16[8,2,24,256]{3,2,1,0:T(8,128)(2,1)} %bitcast.9), calls=%async_computation.1 | async-start | bytes 393216 | tf_op jit(solution)/shard_map/all_to_all | solution.py:172
  195.0 11.1 %all-to-all-start.1 = ((bf16[8,2,6144]{2,1,0:T(2,128)(2,1)}), bf16[8,2,6144]{2,1,0:T(2,128)(2,1)S(1)}, u32[]{:S(2)}, u32[]{:S(2)}) async-start(bf16[8,2,6144]{2,1,0:T(2,128)(2,1)} %reshape.232), calls=%async_computation.2 | async-start | bytes 393216 | tf_op jit(solution)/shard_map/all_to_all | solution.py:194
  198.4 88.9 %all-reduce.7.cloned.1.call-start = ((), (), s32[]{:S(2)}) async-start(), calls=%async_computation.7 | async-start | bytes 131072 | tf_op jit(solution)/shard_map/psum | solution.py:227
  208.2 15.8 %copy-start.19 = (f32[16]{0:T(128)S(1)}, f32[16]{0:T(128)}, u32[]{:S(2)}) copy-start(f32[16]{0:T(128)} %dynamic_slice.35) | copy-start | bytes 196
  208.2 47.7 %copy-start.7 = (bf16[1024,256]{1,0:T(8,128)(2,1)S(1)}, bf16[1024,256]{1,0:T(8,128)(2,1)}, u32[]{:S(2)}) copy-start(bf16[1024,256]{1,0:T(8,128)(2,1)} %param.49) | copy-start | bytes 1572868
  208.2 47.7 %copy-start.14 = (f32[128]{0:T(128)S(1)}, f32[128]{0:T(128)}, u32[]{:S(2)}) copy-start(f32[128]{0:T(128)} %get-tuple-element.19) | copy-start | bytes 1540
  208.2 79.1 %copy-start.3 = (bf16[128,256]{1,0:T(8,128)(2,1)S(1)}, bf16[128,256]{1,0:T(8,128)(2,1)}, u32[]{:S(2)}) copy-start(bf16[128,256]{1,0:T(8,128)(2,1)} %copy-done.2) | copy-start | bytes 196612
  (7 other events, 37.2 us)
Sparse Core Ops, SparseCore 0:
  12.6 65.3 reduce-scatter.2
  125.0 30.7 all-reduce.4
  159.2 64.7 reduce-scatter.4
  256.8 30.3 all-reduce.6
where the time goes:
time: 296 us; the launch traced here: 295 us
  waiting for transfers between devices  110 us (37%)
  blocking collectives  107 us (36%)
  matrix products  23 us (8%)
  local copies, waits for them, and re-layouts  21 us (7%)
  between operations  14.4 us (5%)
  other arithmetic  10.8 us (4%)
  starting transfers between devices  9.25 us (3%)
    all_gather x1, blocking collectives, on_device(): lax.all_gather(dense_hidden, 'ep', axis=0, tiled=True)  30.9 us
    psum x1, waiting for transfers between devices, on_device(): attn_out = lax.psum(attn_part, 'tp')  30.6 us
    psum x1, waiting for transfers between devices, on_device(): lax.psum((routed + mix_share[:, None] * dense_part).astype(jnp.bfloat16),...  30.5 us
    all_gather x1, blocking collectives, on_device(): lax.all_gather(heads_out, 'ep', axis=0, tiled=True)  30.5 us
    reduce_scatter x1, waiting for transfers between devices, on_device(): lax.psum_scatter(jnp.concatenate([jnp.dot(selected, query_weight, preferr...  30.2 us
    psum x1, blocking collectives, on_device(): lax.psum((jnp.sum(stream * stream, axis=1), jnp.dot(normed_in, forget_row...  23.6 us
    psum x1, blocking collectives, on_device(): lax.psum((jnp.sum(middle * middle, axis=1), mix_part), 'ep')  21.9 us
    reduce_scatter x1, waiting for transfers between devices, on_device(): lax.psum_scatter(jnp.concatenate([jnp.dot(selected, dense_gate, preferred...  13.5 us
  transfers between devices with their start and end apart: 6, of which 5 were waited for; matrix products, arithmetic and copies ran while one was open for 9% of the time, Pallas kernels for 0%

commit v1 on v0

--- a/solution.py
+++ b/solution.py
@@ -9,6 +9,12 @@
 TOPK = 2
 CAPACITY = 24
 EPS = 1e-06
+
+
+def gather_and_add(shard, mesh_axis):
+    parts = lax.all_gather(shard, mesh_axis, axis=0, tiled=False)
+    total = parts.sum(axis=0)
+    return total
 
 
 def head_norm(projected, gain_vec):
@@ -146,7 +152,7 @@
         output_weight,
         preferred_element_type=jnp.float32,
     )
-    attn_out = lax.psum(attn_part, "tp")
+    attn_out = gather_and_add(attn_part, "tp")
     middle = (stream + attn_out).astype(jnp.bfloat16).astype(jnp.float32)
     normed_mid = (middle * lax.dynamic_slice_in_dim(ffn_gain, col_start, width_block)).astype(
         jnp.bfloat16

time: 296 us -> 269 us (0.909)
  waiting for transfers between devices: 110 us -> 79.8 us
  blocking collectives: 107 us -> 114 us
    psum x1 -> x0, waiting for transfers between devices: 30.6 us -> none  [on_device(): attn_out = lax.psum(attn_part, 'tp')]
    all_gather x0 -> x1, blocking collectives: none -> 7.13 us  [gather_and_add(): parts = lax.all_gather(shard, mesh_axis, axis=0, tiled=False)]
    unnamed x54 -> x46, local copies, waits for them, and re-layouts: 9.15 us -> 9.7 us
  transfers between devices with their start and end apart: 6 -> 5, of which waited for: 5 -> 4; matrix products, arithmetic and copies ran while one was open for 9% -> 10% of each run, Pallas kernels for 0% -> 0%
where the time goes in v1:
time: 269 us; the launch traced here: 268 us
  blocking collectives  114 us (42%)
  waiting for transfers between devices  79.8 us (30%)
  matrix products  22.7 us (8%)
  local copies, waits for them, and re-layouts  19.6 us (7%)
  between operations  14.3 us (5%)
  other arithmetic  10 us (4%)
  starting transfers between devices  7.35 us (3%)
    all_gather x1, blocking collectives, on_device(): lax.all_gather(dense_hidden, 'ep', axis=0, tiled=True)  30.9 us
    reduce_scatter x1, waiting for transfers between devices, on_device(): lax.psum_scatter(jnp.concatenate([jnp.dot(selected, query_weight, preferr...  30.7 us
    all_gather x1, blocking collectives, on_device(): lax.all_gather(heads_out, 'ep', axis=0, tiled=True)  30.7 us
    psum x1, waiting for transfers between devices, on_device(): lax.psum((routed + mix_share[:, None] * dense_part).astype(jnp.bfloat16),...  30.6 us
    psum x1, blocking collectives, on_device(): lax.psum((jnp.sum(stream * stream, axis=1), jnp.dot(normed_in, forget_row...  23.9 us
    psum x1, blocking collectives, on_device(): lax.psum((jnp.sum(middle * middle, axis=1), mix_part), 'ep')  21.9 us
    reduce_scatter x1, waiting for transfers between devices, on_device(): lax.psum_scatter(jnp.concatenate([jnp.dot(selected, dense_gate, preferred...  13.4 us
    unnamed x46, local copies, waits for them, and re-layouts  9.7 us
  transfers between devices with their start and end apart: 5, of which 4 were waited for; matrix products, arithmetic and copies ran while one was open for 10% of the time, Pallas kernels for 0%

profile of v1, /device:TPU:0, one launch (start us, length us, event | category | flops | bytes accessed | tf_op | source)
XLA Modules:
  0.0 268.2 jit_solution(12008794366943263261)
XLA Ops:
  8.2 1.2 fusion.40
  10.5 1.1 fusion.38
  12.8 4.7 %copy.71 = f32[16,4,1024]{1,2,0:T(8,128)} copy(f32[16,4,1024]{2,1,0:T(4,128)S(1)} %copy-done.4) | data formatting | bytes 524288 | tf_op args[11]
  18.9 23.9 %all-reduce.1 = (f32[128,16]{0,1:T(8,128)S(1)}, f32[128]{0:T(128)S(1)}) all-reduce(f32[128,16]{0,1:T(8,128)S(1)} %fusion.34, f32[128]{0:T(128)S(1)} %fusion.15), channel_id=1, replica_groups=mesh['ep'=8,'tp'=4] {'ep'}, use_global_device_ids=true, to_apply=%region_2.0 | all-reduce | flops 2176 | bytes 17408 | tf_op jit(solution)/shard_map/psum | solution.py:76
  42.9 1.3 gather_fusion.1
  47.4 30.7 %reduce-scatter.3.cloned.1.call-done = f32[16,1024]{1,0:T(8,128)} async-done(((f32[128,1024]{1,0:T(8,128)}), f32[16,1024]{1,0:T(8,128)}) %reduce-scatter.3.cloned.1.call-update) | async-done | bytes 65552 | tf_op jit(solution)/shard_map/reduce_scatter | solution.py:87
  80.4 5.8 %fusion.64 = (f32[16,2,2]{2,1,0:T(2,128)S(1)}, f32[16,2,2,1024]{3,2,1,0:T(2,128)S(1)}) fusion(f32[16,2,2,1024]{3,2,1,0:T(2,128)S(1)} %reshape.201, f32[16,2,2]{2,1,0:T(2,128)S(1)} %copy.73, bf16[16,2,2,128]{3,2,1,0:T(2,128)(2,1)S(1)} %multiply_convert_fusion, bf16[16,2,1024,128]{3,2,1,0:T(8,128)(2,1)} %param.34, pred[16,1024]{1,0:T(8,128)(4,1)S(1)} %iota_compare_fusion.1), kind=kOutput, calls=%fused_computation.109 | convolution fusion | flops 17104832 | bytes 8946176 | tf_op jit(solution)/shard_map/skgd,skcd->skgc/dot_general | solution.py:122
  87.8 4.7 %fusion.9 = bf16[16,2,2,128]{3,2,1,0:T(2,128)(2,1)S(1)} fusion(bf16[16,2,1024,128]{3,2,1,0:T(8,128)(2,1)} %param.35, f32[16,2,2,1024]{3,2,1,0:T(2,128)S(1)} %get-tuple-element.22, f32[16,2,2]{2,1,0:T(2,128)S(1)} %multiply_maximum_fusion, f32[16,2,2]{2,1,0:T(2,128)S(1)} %get-tuple-element.13, f32[16,2,128]{2,1,0:T(2,128)S(1)} %reshape.207, ...), kind=kOutput, calls=%fused_computation.18 | convolution fusion | flops 16941056 | bytes 8684288 | tf_op jit(solution)/shard_map/skgc,skcd->skgd/dot_general | solution.py:138
  92.6 30.7 %all_gather.12 = bf16[128,512]{1,0:T(8,128)(2,1)S(1)} all-gather(bf16[16,512]{1,0:T(8,128)(2,1)S(1)} %convert_element_type.102), channel_id=1, replica_groups=mesh['ep'=8,'tp'=4] {'ep'}, dimensions={0}, use_global_device_ids=true | all-gather | bytes 147456 | tf_op jit(solution)/shard_map/all_gather | solution.py:151
  123.4 7.1 %all-gather = f32[512,256]{1,0:T(8,128)S(1)} all-gather(f32[128,256]{1,0:T(8,128)S(1)} %fusion.65), channel_id=2, replica_groups=mesh['ep'=8,'tp'=4] {'tp'}, dimensions={0}, use_global_device_ids=true | all-gather | bytes 655360 | tf_op jit(solution)/shard_map/all_gather | solution.py:15
  131.0 1.3 fusion.30
  134.3 3.7 %all-to-all-start = ((bf16[8,2,24,256]{3,2,1,0:T(8,128)(2,1)}), bf16[8,2,24,256]{3,2,1,0:T(8,128)(2,1)S(1)}, u32[]{:S(2)}, u32[]{:S(2)}) async-start(bf16[8,2,24,256]{3,2,1,0:T(8,128)(2,1)} %bitcast.10), calls=%async_computation.1 | async-start | bytes 393216 | tf_op jit(solution)/shard_map/all_to_all | solution.py:178
  138.1 21.9 %all-reduce = (f32[128]{0:T(128)S(1)}, f32[128]{0:T(128)S(1)}) all-reduce(f32[128]{0:T(128)S(1)} %get-tuple-element.11, f32[128]{0:T(128)S(1)} %convolution_bitcast_fusion), channel_id=1, replica_groups=mesh['ep'=8,'tp'=4] {'ep'}, use_global_device_ids=true, to_apply=%region_14.15 | all-reduce | flops 256 | bytes 2048 | tf_op jit(solution)/shard_map/psum | solution.py:165
  160.9 1.9 convolution_multiply_fusion.3
  162.9 2.3 fusion
  166.0 2.0 reshape.233
  168.0 3.4 %all-to-all-start.1 = ((bf16[8,2,6144]{2,1,0:T(2,128)(2,1)}), bf16[8,2,6144]{2,1,0:T(2,128)(2,1)S(1)}, u32[]{:S(2)}, u32[]{:S(2)}) async-start(bf16[8,2,6144]{2,1,0:T(2,128)(2,1)} %reshape.233), calls=%async_computation.2 | async-start | bytes 393216 | tf_op jit(solution)/shard_map/all_to_all | solution.py:200
  174.0 5.2 %all-to-all-done.1 = bf16[8,2,6144]{2,1,0:T(2,128)(2,1)S(1)} async-done(((bf16[8,2,6144]{2,1,0:T(2,128)(2,1)}), bf16[8,2,6144]{2,1,0:T(2,128)(2,1)S(1)}, u32[]{:S(2)}, u32[]{:S(2)}) %all-to-all-start.1) | async-done | bytes 196640 | tf_op jit(solution)/shard_map/all_to_all | solution.py:200
  179.2 1.5 reshape.234
  181.2 1.2 gather_fusion
  183.5 13.4 %reduce-scatter.5.cloned.1.call-done = f32[16,2048]{1,0:T(8,128)} async-done(((f32[128,2048]{1,0:T(8,128)}), f32[16,2048]{1,0:T(8,128)}) %reduce-scatter.5.cloned.1.call-update) | async-done | bytes 131088 | tf_op jit(solution)/shard_map/reduce_scatter | solution.py:210
  197.9 30.9 %all_gather.15 = bf16[128,1024]{1,0:T(8,128)(2,1)S(1)} all-gather(bf16[16,1024]{1,0:T(8,128)(2,1)S(1)} %fusion.22), channel_id=1, replica_groups=mesh['ep'=8,'tp'=4] {'ep'}, dimensions={0}, use_global_device_ids=true | all-gather | bytes 294912 | tf_op jit(solution)/shard_map/all_gather | solution.py:229
  229.6 30.6 %all-reduce.4.cloned.1.call-done = bf16[128,256]{1,0:T(8,128)(2,1)} async-done(((bf16[128,256]{1,0:T(8,128)(2,1)}), bf16[128,256]{1,0:T(8,128)(2,1)}) %all-reduce.4.cloned.1.call-update) | async-done | bytes 65552 | tf_op jit(solution)/shard_map/psum | solution.py:233
  260.2 1.5 fusion.19
  (130 shorter events, 22.2 us)
Async XLA Ops:
  7.2 155.7 %copy-start = (bf16[2,256,2048]{2,1,0:T(8,128)(2,1)S(1)}, bf16[2,256,2048]{2,1,0:T(8,128)(2,1)}, u32[]{:S(2)}) copy-start(bf16[2,256,2048]{2,1,0:T(8,128)(2,1)} %param.45) | copy-start | bytes 6291460
  7.2 5.4 %copy-start.1 = (bf16[128,256]{1,0:T(8,128)(2,1)S(1)}, bf16[128,256]{1,0:T(8,128)(2,1)}, u32[]{:S(2)}) copy-start(bf16[128,256]{1,0:T(8,128)(2,1)} %param.25) | copy-start | bytes 196612
  7.2 5.5 %copy-start.17 = (s32[16]{0:T(128)S(1)}, s32[16]{0:T(128)}, u32[]{:S(2)}) copy-start(s32[16]{0:T(128)} %param.37) | copy-start | bytes 196
  7.2 5.5 %copy-start.4 = (f32[16,4,1024]{2,1,0:T(4,128)S(1)}, f32[16,4,1024]{2,1,0:T(4,128)}, u32[]{:S(2)}) copy-start(f32[16,4,1024]{2,1,0:T(4,128)} %param.36) | copy-start | bytes 786436
  7.2 70.8 %reduce-scatter.3.cloned.1.call-start = ((), (), s32[]{:S(2)}) async-start(), calls=%async_computation.4 | async-start | bytes 589824 | tf_op jit(solution)/shard_map/reduce_scatter | solution.py:87
  12.5 184.4 %reduce-scatter.5.cloned.1.call-start = ((), (), s32[]{:S(2)}) async-start(), calls=%async_computation.5 | async-start | bytes 1179648 | tf_op jit(solution)/shard_map/reduce_scatter | solution.py:210
  12.7 4.9 %copy-start.18 = (s32[128]{0:T(128)S(1)}, s32[128]{0:T(128)}, u32[]{:S(2)}) copy-start(s32[128]{0:T(128)} %param.40) | copy-start | bytes 1540
  12.7 4.9 %copy-start.13 = (s32[128,2]{0,1:T(2,128)S(1)}, s32[128,2]{0,1:T(2,128)}, u32[]{:S(2)}) copy-start(s32[128,2]{0,1:T(2,128)} %param.41) | copy-start | bytes 3076
  12.7 31.6 %copy-start.19 = (f32[16]{0:T(128)S(1)}, f32[16]{0:T(128)}, u32[]{:S(2)}) copy-start(f32[16]{0:T(128)} %param.28) | copy-start | bytes 196
  12.8 34.5 %copy-start.14 = (f32[128]{0:T(128)S(1)}, f32[128]{0:T(128)}, u32[]{:S(2)}) copy-start(f32[128]{0:T(128)} %param.33) | copy-start | bytes 1540
  12.8 67.3 %copy-start.15 = (f32[128]{0:T(128)S(1)}, f32[128]{0:T(128)}, u32[]{:S(2)}) copy-start(f32[128]{0:T(128)} %param.32) | copy-start | bytes 1540
  80.3 6.3 %copy-start.9 = (f32[16,1024]{1,0:T(8,128)S(1)}, f32[16,1024]{1,0:T(8,128)}, u32[]{:S(2)}) copy-start(f32[16,1024]{1,0:T(8,128)} %reduce-scatter.3.cloned.1.call-done) | copy-start | bytes 196612
  87.8 35.4 %copy-start.7 = (bf16[512,256]{1,0:T(8,128)(2,1)S(1)}, bf16[512,256]{1,0:T(8,128)(2,1)}, u32[]{:S(2)}) copy-start(bf16[512,256]{1,0:T(8,128)(2,1)} %param.38) | copy-start | bytes 786436
  92.5 38.2 %copy-start.5 = (bf16[256,1024]{1,0:T(8,128)(2,1)S(1)}, bf16[256,1024]{1,0:T(8,128)(2,1)}, u32[]{:S(2)}) copy-start(bf16[256,1024]{1,0:T(8,128)(2,1)} %param.48) | copy-start | bytes 1572868
  130.7 7.2 %copy-start.2 = (bf16[128,256]{1,0:T(8,128)(2,1)}, bf16[128,256]{1,0:T(8,128)(2,1)S(1)}, u32[]{:S(2)}) copy-start(bf16[128,256]{1,0:T(8,128)(2,1)S(1)} %get-tuple-element.12) | copy-start | bytes 196612
  134.3 26.5 %all-to-all-start = ((bf16[8,2,24,256]{3,2,1,0:T(8,128)(2,1)}), bf16[8,2,24,256]{3,2,1,0:T(8,128)(2,1)S(1)}, u32[]{:S(2)}, u32[]{:S(2)}) async-start(bf16[8,2,24,256]{3,2,1,0:T(8,128)(2,1)} %bitcast.10), calls=%async_computation.1 | async-start | bytes 393216 | tf_op jit(solution)/shard_map/all_to_all | solution.py:178
  165.3 6.8 %copy-start.12 = (f32[128,2]{0,1:T(2,128)S(1)}, f32[128,2]{0,1:T(2,128)}, u32[]{:S(2)}) copy-start(f32[128,2]{0,1:T(2,128)} %param.42) | copy-start | bytes 3076
  168.0 11.1 %all-to-all-start.1 = ((bf16[8,2,6144]{2,1,0:T(2,128)(2,1)}), bf16[8,2,6144]{2,1,0:T(2,128)(2,1)S(1)}, u32[]{:S(2)}, u32[]{:S(2)}) async-start(bf16[8,2,6144]{2,1,0:T(2,128)(2,1)} %reshape.233), calls=%async_computation.2 | async-start | bytes 393216 | tf_op jit(solution)/shard_map/all_to_all | solution.py:200
  171.4 88.8 %all-reduce.4.cloned.1.call-start = ((), (), s32[]{:S(2)}) async-start(), calls=%async_computation.6 | async-start | bytes 131072 | tf_op jit(solution)/shard_map/psum | solution.py:233
  181.2 1.5 copy-start.8
  181.2 15.7 %copy-start.16 = (f32[16]{0:T(128)S(1)}, f32[16]{0:T(128)}, u32[]{:S(2)}) copy-start(f32[16]{0:T(128)} %dynamic_slice.35) | copy-start | bytes 196
  181.2 47.5 %copy-start.6 = (bf16[1024,256]{1,0:T(8,128)(2,1)S(1)}, bf16[1024,256]{1,0:T(8,128)(2,1)}, u32[]{:S(2)}) copy-start(bf16[1024,256]{1,0:T(8,128)(2,1)} %param.49) | copy-start | bytes 1572868
  181.2 47.5 %copy-start.11 = (f32[128]{0:T(128)S(1)}, f32[128]{0:T(128)}, u32[]{:S(2)}) copy-start(f32[128]{0:T(128)} %get-tuple-element.19) | copy-start | bytes 1540
  181.2 79.0 %copy-start.3 = (bf16[128,256]{1,0:T(8,128)(2,1)S(1)}, bf16[128,256]{1,0:T(8,128)(2,1)}, u32[]{:S(2)}) copy-start(bf16[128,256]{1,0:T(8,128)(2,1)} %copy-done.2) | copy-start | bytes 196612
  (1 other events, 0.6 us)
Sparse Core Ops, SparseCore 0:
  12.6 65.3 reduce-scatter.2
  133.5 63.3 reduce-scatter.4
  229.7 30.4 all-reduce.3
